TPU v7x, 32 devices: a whole 2x2x4 slice. The times are simulated.
32 devices in a mesh: fs: 8 (over z, y), tp: 4 (over x, core).
Axes of the slice: x: 2, y: 2, z: 4, core: 2. Of those that a mesh axis runs over, the one named last changes fastest.
Arguments:
- inputs: bfloat16 [2048, 2048], P('fs', 'tp'), may hold values from -6 to 6
- cotangent: bfloat16 [2048, 2048], P('fs', 'tp'), may hold values from -8 to 8
- gate_weight: bfloat16 [2048, 5632], P('fs', 'tp'), may hold values from -0.125 to 0.125
- up_weight: bfloat16 [2048, 5632], P('fs', 'tp'), may hold values from -0.125 to 0.125
- down_weight: bfloat16 [5632, 2048], P('tp', 'fs'), may hold values from -0.078125 to 0.078125
Outputs:
- grad_inputs: bfloat16 [2048, 2048], P('fs', 'tp')
- grad_gate: float32 [2048, 5632], P('fs', 'tp')
- grad_up: float32 [2048, 5632], P('fs', 'tp')
- grad_down: float32 [5632, 2048], P('tp', 'fs')
All inputs are finite; a program needn't handle non-finite values.
Results may differ from a plain program's by a relative error of at most 0.015.
Values may be sent and summed in bfloat16 or wider, within the bound.
A program may use at most 64 MiB of HBM per device.

v0:
```python
import functools

import jax
import jax.numpy as jnp
from jax import lax
from jax.experimental import pallas as pl
from jax.experimental.pallas import tpu as pltpu
from jax.sharding import PartitionSpec as P

MESH = pl.DeviceIdType.MESH
ANY = pl.BlockSpec(memory_space=pl.ANY)
VMEM = pl.BlockSpec(memory_space=pltpu.VMEM)
CORES = 2


def contract_rows(left, right):
    return lax.dot_general(
        left, right, (((0,), (0,)), ((), ())), preferred_element_type=jnp.float32
    )


def contract_cols(left, right):
    return lax.dot_general(
        left, right, (((1,), (1,)), ((), ())), preferred_element_type=jnp.float32
    )


def gathered_plan(inputs, cotangent, gate_weight, up_weight, down_weight):
    whole_inputs = lax.all_gather(inputs, "tp", axis=1, tiled=True)
    whole_cotangent = lax.all_gather(cotangent, "tp", axis=1, tiled=True)
    gate_whole = lax.all_gather(gate_weight, "fs", axis=0, tiled=True)
    up_whole = lax.all_gather(up_weight, "fs", axis=0, tiled=True)
    down_whole = lax.all_gather(down_weight, "fs", axis=1, tiled=True)
    gate_pre = jnp.dot(whole_inputs, gate_whole, preferred_element_type=jnp.float32)
    up_pre = jnp.dot(whole_inputs, up_whole, preferred_element_type=jnp.float32)
    grad_hidden = contract_cols(whole_cotangent, down_whole)
    hidden, grad_gate_pre, grad_up_pre = pointwise(gate_pre, up_pre, grad_hidden)
    pre_grads = jnp.concatenate([grad_gate_pre, grad_up_pre], axis=1)
    width = gate_weight.shape[1]
    partial_sum = contract_cols(grad_gate_pre, gate_whole) + contract_cols(grad_up_pre, up_whole)

    def scattered(values, axis, dim):
        return lax.psum_scatter(
            values.astype(jnp.bfloat16), axis, scatter_dimension=dim, tiled=True
        )

    grad_inputs = scattered(partial_sum, "tp", 1)
    expand = scattered(contract_rows(whole_inputs, pre_grads), "fs", 0).astype(jnp.float32)
    down = scattered(contract_rows(whole_cotangent, hidden), "fs", 0).astype(jnp.float32)
    return (grad_inputs, expand[:, :width], expand[:, width:], down.T)


def pointwise(gate_pre, up_pre, grad_hidden):
    gate_sig = jax.nn.sigmoid(gate_pre)
    gate_act = gate_pre * gate_sig
    hidden = (gate_act * up_pre).astype(jnp.bfloat16)
    grad_gate_pre = (grad_hidden * up_pre * gate_sig * (1.0 + gate_pre * (1.0 - gate_sig))).astype(
        jnp.bfloat16
    )
    grad_up_pre = (grad_hidden * gate_act).astype(jnp.bfloat16)
    return hidden, grad_gate_pre, grad_up_pre


def block(index, size):
    return pl.ds(pl.multiple_of(index * size, size), size)


class Place:
    def __init__(self, nz, ny, nx):
        self.nz, self.ny, self.nx = nz, ny, nx
        fs, tp = lax.axis_index("fs"), lax.axis_index("tp")
        self.fs, self.tp = fs, tp
        self.z, self.y = fs // ny, fs % ny
        self.x, self.c = tp // CORES, tp % CORES

    def by_z(self, dz):
        return {"fs": ((self.z + dz) % self.nz) * self.ny + self.y, "tp": self.tp}

    def by_y(self, dy):
        return {"fs": self.z * self.ny + (self.y + dy) % self.ny, "tp": self.tp}

    def by_x(self, dx):
        return {"fs": self.fs, "tp": ((self.x + dx) % self.nx) * CORES + self.c}

    def by_core(self):
        return {"fs": self.fs, "tp": self.x * CORES + 1 - self.c}

    def by_tp(self, dt):
        return {"fs": self.fs, "tp": (self.tp + dt) % (self.nx * CORES)}


def meet(partners):
    barrier = pltpu.get_barrier_semaphore()
    for partner in partners:
        pl.semaphore_signal(barrier, inc=1, device_id=partner, device_id_type=MESH)
    pl.semaphore_wait(barrier, len(partners))


class Copies:
    def __init__(self, send_sem, recv_sem):
        self.send_sem, self.recv_sem, self.made = send_sem, recv_sem, []

    def start(self, source, target, device):
        at = len(self.made)
        copy = pltpu.make_async_remote_copy(
            src_ref=source, dst_ref=target, send_sem=self.send_sem.at[at],
            recv_sem=self.recv_sem.at[at], device_id=device, device_id_type=MESH,
        )
        copy.start()
        self.made.append(copy)
        return copy


def flip(value, mask, nz):
    bit = 1
    while bit < nz:
        if mask & bit:
            value = value + bit - 2 * bit * ((value // bit) % 2)
        bit *= 2
    return value


def far_first(nz):
    return sorted(range(1, nz), key=lambda d: -min(d, nz - d))


def gather_kernel(sizes, x_ref, c_ref, *refs):
    nz, ny, nx = sizes
    me = Place(*sizes)
    w_refs, (xf, cf, *wfs) = refs[:3], refs[3:8]
    send_sem, recv_sem, own_sem = refs[8:]
    tokens, features = x_ref.shape
    depth, units = w_refs[0].shape[1], w_refs[0].shape[0] // nz
    bits = [1 << at for at in reversed(range(nz.bit_length() - 1))]
    meet(
        [me.by_z(d) for d in range(1, nz)]
        + [me.by_y(d) for d in range(1, ny)]
        + [me.by_x(d) for d in range(1, nx)]
        + [me.by_core()]
    )
    copies = Copies(send_sem, recv_sem)
    wholes = (xf, cf)
    by_x, sent_z, w_sent, last = {}, {}, {}, []

    def spot(whole, mask, tp):
        return whole.at[block(flip(me.z, mask, nz), tokens), block(tp, features)]

    def w_spot(whole, dz):
        return whole.at[:, block(((me.z - dz + nz) % nz) * ny + me.y, depth)]

    def held(mask):
        return (x_ref, c_ref) if mask == 0 else [spot(whole, mask, me.tp) for whole in wholes]

    def pass_z(bit, mask):
        there = {"fs": flip(me.z, bit, nz) * ny + me.y, "tp": me.tp}
        sent_z[bit, mask] = [
            copies.start(source, spot(whole, mask, me.tp), there)
            for source, whole in zip(held(mask), wholes)
        ]

    def pass_tp(mask):
        for dx in range(1, nx):
            by_x[mask, dx] = [
                copies.start(source, spot(whole, mask, me.tp), me.by_x(dx))
                for source, whole in zip(held(mask), wholes)
            ]
        for source, whole in zip(held(mask), wholes):
            last.append(copies.start(source, spot(whole, mask, me.tp), me.by_core()))

    def pass_core(mask):
        for dx in range(1, nx):
            tp = ((me.x - dx + nx) % nx) * CORES + me.c
            for copy, whole in zip(by_x[mask, dx], wholes):
                copy.wait_recv()
                here = spot(whole, mask, tp)
                last.append(copies.start(here, here, me.by_core()))

    def send_w(dz):
        w_sent[dz] = [
            copies.start(w.at[block((me.z + dz) % nz, units), :], w_spot(wf, 0), me.by_z(dz))
            for w, wf in zip(w_refs, wfs)
        ]

    for bit in bits:
        pass_z(bit, 0)
    pass_tp(0)
    order = far_first(nz)
    send_w(order[0])
    own = []
    for w, wf in zip(w_refs, wfs):
        mine = w.at[block(me.z, units), :]
        last += [copies.start(mine, w_spot(wf, 0), me.by_y(dy)) for dy in range(1, ny)]
        own.append((mine, w_spot(wf, 0)))
    own += [(x_ref, spot(xf, 0, me.tp)), (c_ref, spot(cf, 0, me.tp))]
    own = [pltpu.make_async_copy(*pair, own_sem.at[at]) for at, pair in enumerate(own)]
    for copy in own:
        copy.start()
    masks = [0]
    for at, bit in enumerate(bits):
        for mask in list(masks):
            for copy in sent_z[bit, mask]:
                copy.wait_recv()
            masks.append(mask + bit)
            for lower in bits[at + 1 :]:
                pass_z(lower, mask + bit)
            pass_tp(mask + bit)
        if at == 0:
            for dz in order[1:]:
                send_w(dz)
    for at, dz in enumerate(order):
        for copy, wf in zip(w_sent[dz], wfs):
            copy.wait_recv()
            here = w_spot(wf, dz)
            last += [copies.start(here, here, me.by_y(dy)) for dy in range(1, ny)]
        pass_core(masks[at])
    pass_core(masks[-1])
    for copy in last:
        copy.wait_recv()
    for copy in copies.made:
        copy.wait_send()
    for copy in own:
        copy.wait()


def reduce_kernel(sizes, *refs):
    nz, ny, nx = sizes
    me = Place(*sizes)
    n_tp = nx * CORES
    g_refs, i_ref, r, out = refs[:3], refs[3], refs[4], refs[5]
    rg, sg, ri, si, rz, send_sem, recv_sem, own_sem = refs[6:]
    units, depth = rg.shape[3:]
    tokens, features = rz.shape[1:]
    meet(
        [me.by_y(d) for d in range(1, ny)]
        + [me.by_tp(d) for d in range(1, n_tp)]
        + [me.by_z(d) for d in range(1, nz)]
    )
    copies = Copies(send_sem, recv_sem)
    order = far_first(nz) + [0]
    by_y, by_tp = {}, {}
    for dz in order:
        there = (me.z + dz) % nz
        for at, g in enumerate(g_refs):
            by_y[dz, at] = [
                copies.start(
                    g.at[:, block(there * ny + (me.y + dy) % ny, depth)],
                    rg.at[dy - 1, dz, at],
                    me.by_y(dy),
                )
                for dy in range(1, ny)
            ]
        by_tp[dz] = [
            copies.start(
                i_ref.at[block(there, tokens), block((me.tp + dt) % n_tp, features)],
                ri.at[dt - 1, dz],
                me.by_tp(dt),
            )
            for dt in range(1, n_tp)
        ]
    final, waiting = [], []

    def release():
        while waiting:
            final.append(copies.start(*waiting.pop(0)))

    for dz in order:
        there = (me.z + dz) % nz
        for at, g in enumerate(g_refs):
            total = g[:, block(there * ny + me.y, depth)].astype(jnp.float32)
            for dy, copy in enumerate(by_y[dz, at]):
                copy.wait_recv()
                total += rg[dy, dz, at].astype(jnp.float32)
            sg[dz, at] = total.astype(jnp.bfloat16)
            release()
            if dz:
                target = r.at[at, block(me.z, units), :]
                waiting.append((sg.at[dz, at], target, me.by_z(dz)))
    for dz in order:
        rows = block((me.z + dz) % nz, tokens)
        total = i_ref[rows, block(me.tp, features)].astype(jnp.float32)
        for dt, copy in enumerate(by_tp[dz]):
            copy.wait_recv()
            total += ri[dt, dz].astype(jnp.float32)
        si[dz] = total.astype(si.dtype)
        release()
        if dz:
            waiting.append((si.at[dz], rz.at[dz - 1], me.by_z(dz)))
    own = pltpu.make_async_copy(sg.at[0], r.at[:, block(me.z, units), :], own_sem)
    own.start()
    for copy in final:
        copy.wait_recv()
    total = si[0].astype(jnp.float32)
    for dz in range(1, nz):
        total += rz[dz - 1].astype(jnp.float32)
    out[...] = total.astype(out.dtype)
    for copy in copies.made:
        copy.wait_send()
    own.wait()


def split_plan(sizes, inputs, cotangent, gate_weight, up_weight, down_weight):
    nz, ny, nx = sizes
    n_tp = nx * CORES
    tokens, features = inputs.shape
    depth, width = gate_weight.shape
    units, rows, model = width // nz, tokens * nz, depth * nz * ny
    dma, half = pltpu.SemaphoreType.DMA, jnp.bfloat16
    count = 2 * (nz * (nx - 1) + nz * nx + nz - 1) + 3 * (nz - 1) + 3 * nz * (ny - 1)
    all_x, all_c, gate_whole, up_whole, down_whole = pl.pallas_call(
        functools.partial(gather_kernel, sizes),
        out_shape=[jax.ShapeDtypeStruct((rows, model), half)] * 2
        + [jax.ShapeDtypeStruct((units, model), half)] * 3,
        in_specs=[VMEM] * 5,
        out_specs=[ANY] * 5,
        scratch_shapes=[dma((count,)), dma((count,)), dma((5,))],
        compiler_params=pltpu.CompilerParams(collective_id=0, has_side_effects=True),
    )(inputs, cotangent, gate_weight.T, up_weight.T, down_weight)
    gate_pre = contract_cols(all_x, gate_whole)
    up_pre = contract_cols(all_x, up_whole)
    grad_hidden = contract_cols(all_c, down_whole)
    hidden, grad_gate_pre, grad_up_pre = pointwise(gate_pre, up_pre, grad_hidden)
    partial = jnp.dot(grad_gate_pre, gate_whole, preferred_element_type=jnp.float32) + jnp.dot(
        grad_up_pre, up_whole, preferred_element_type=jnp.float32
    )
    count = nz * (3 * (ny - 1) + n_tp - 1) + 4 * (nz - 1)
    settled, grad_inputs = pl.pallas_call(
        functools.partial(reduce_kernel, sizes),
        out_shape=[
            jax.ShapeDtypeStruct((3, width, depth), half),
            jax.ShapeDtypeStruct((tokens, features), half),
        ],
        in_specs=[VMEM] * 4,
        out_specs=[ANY, VMEM],
        scratch_shapes=[
            pltpu.VMEM((ny - 1, nz, 3, units, depth), half),
            pltpu.VMEM((nz, 3, units, depth), half),
            pltpu.VMEM((n_tp - 1, nz, tokens, features), half),
            pltpu.VMEM((nz, tokens, features), half),
            pltpu.VMEM((nz - 1, tokens, features), half),
            dma((count,)),
            dma((count,)),
            dma,
        ],
        compiler_params=pltpu.CompilerParams(collective_id=1, has_side_effects=True),
    )(
        contract_rows(grad_gate_pre, all_x).astype(half),
        contract_rows(grad_up_pre, all_x).astype(half),
        contract_rows(hidden, all_c).astype(half),
        partial.astype(half),
    )
    return (
        grad_inputs,
        settled[0].T.astype(jnp.float32),
        settled[1].T.astype(jnp.float32),
        settled[2].astype(jnp.float32),
    )


def solution(mesh):
    n_fs, n_tp = mesh.shape["fs"], mesh.shape["tp"]
    nx = max(1, n_tp // CORES)
    ny = nx
    nz = n_fs // ny

    def per_device(inputs, cotangent, gate_weight, up_weight, down_weight):
        arrays = (inputs, cotangent, gate_weight, up_weight, down_weight)
        depth, width = gate_weight.shape
        fits = n_tp == nx * CORES and nz > 1 and ny > 1 and n_fs == nz * ny
        fits = fits and nz & (nz - 1) == 0
        tiles = depth % 128 == 0 and inputs.shape[1] % 128 == 0 and inputs.shape[0] % 16 == 0
        if fits and tiles and width % (16 * nz) == 0:
            return split_plan((nz, ny, nx), *arrays)
        return gathered_plan(*arrays)

    return jax.shard_map(
        per_device,
        mesh=mesh,
        in_specs=(P("fs", "tp"), P("fs", "tp"), P("fs", "tp"), P("fs", "tp"), P("tp", "fs")),
        out_specs=(P("fs", "tp"), P("fs", "tp"), P("fs", "tp"), P("tp", "fs")),
        check_vma=False,
    )
```

profile of v0, /device:TPU:0, one launch (start us, length us, event | category | flops | bytes accessed | tf_op | source)
XLA Modules:
  0.0 205.3 jit_solution(2690535426892039590)
XLA Ops:
  0.6 0.0 copy-start.2
  0.6 2.3 %copy.9 = bf16[256,1408]{0,1:T(8,128)(2,1)} copy(bf16[256,1408]{1,0:T(8,128)(2,1)} %param.7) | data formatting | bytes 1441792 | tf_op args[2]
  3.0 0.0 copy-done.2
  3.0 1.1 copy.10
  4.1 89.8 %shard_map.84 = (bf16[1024,2048]{1,0:T(8,128)(2,1)}, bf16[1024,2048]{1,0:T(8,128)(2,1)}, bf16[352,2048]{1,0:T(8,128)(2,1)}, bf16[352,2048]{1,0:T(8,128)(2,1)}, bf16[352,2048]{1,0:T(8,128)(2,1)}) custom-call(bf16[256,512]{1,0:T(8,128)(2,1)} %x_ref.1, bf16[256,512]{1,0:T(8,128)(2,1)} %c_ref.1, bf16[1408,256]{1,0:T(8,128)(2,1)} %bitcast.30, ...), custom_call_target="tpu_custom_call" | custom-call | tf_op jit(solution)/shard_map/pallas_call | solution.py:309
  93.9 0.0 copy-start.1
  93.9 0.0 copy-start.4
  93.9 4.5 %fusion.3 = f32[1024,352]{0,1:T(8,128)S(1)} fusion(bf16[1024,2048]{1,0:T(8,128)(2,1)} %get-tuple-element.13, bf16[352,2048]{1,0:T(8,128)(2,1)} %get-tuple-element.14), kind=kOutput, calls=%fused_computation.13 | convolution fusion | flops 1476395008 | bytes 7077888 | tf_op jit(solution)/shard_map/dot_general | solution.py:23
  98.4 0.0 copy-done.1
  98.4 0.0 copy-done.4
  98.4 0.0 copy-start.5
  98.4 0.0 copy-start.6
  98.4 1.7 fusion.4
  100.1 0.5 copy-done.5
  100.6 0.4 copy-done.6
  101.0 2.1 %multiply_convert_fusion.1 = (bf16[1024,352]{0,1:T(8,128)(2,1)S(1)}, bf16[1024,352]{0,1:T(8,128)(2,1)S(1)}) fusion(f32[1024,352]{0,1:T(8,128)S(1)} %fusion.4, f32[1024,352]{0,1:T(8,128)S(1)} %fusion.3, bf16[1024,2048]{1,0:T(8,128)(2,1)S(1)} %copy-done.5, bf16[352,2048]{1,0:T(8,128)(2,1)S(1)} %copy-done.6), kind=kOutput, calls=%fused_computation.7 | convolution fusion | flops 1481080832 | bytes 9961472 | tf_op jit(solution)/shard_map/dot_general | solution.py:23
  103.2 2.9 %convolution_convert_fusion.refs_2_ = bf16[352,2048]{1,0:T(8,128)(2,1)} fusion(bf16[1024,2048]{1,0:T(8,128)(2,1)S(1)} %copy-done.5, f32[1024,352]{0,1:T(8,128)S(1)} %fusion.3, f32[1024,352]{0,1:T(8,128)S(1)} %fusion.4), kind=kOutput, calls=%fused_computation.1 | convolution fusion | flops 1479278592 | bytes 8519680 | tf_op jit(solution)/shard_map/dot_general | solution.py:17
  106.1 2.8 %convolution_convert_fusion.1.refs_1_ = bf16[352,2048]{1,0:T(8,128)(2,1)} fusion(bf16[1024,352]{0,1:T(8,128)(2,1)S(1)} %get-tuple-element.22, bf16[1024,2048]{1,0:T(8,128)(2,1)S(1)} %copy-done.4), kind=kOutput, calls=%fused_computation.2 | convolution fusion | flops 1477115904 | bytes 6356992 | tf_op jit(solution)/shard_map/dot_general | solution.py:17
  108.9 2.8 %convolution_convert_fusion.2.refs_0_ = bf16[352,2048]{1,0:T(8,128)(2,1)} fusion(bf16[1024,352]{0,1:T(8,128)(2,1)S(1)} %get-tuple-element.23, bf16[1024,2048]{1,0:T(8,128)(2,1)S(1)} %copy-done.4), kind=kOutput, calls=%fused_computation.3 | convolution fusion | flops 1477115904 | bytes 6356992 | tf_op jit(solution)/shard_map/dot_general | solution.py:17
  111.7 0.0 copy-start
  111.7 2.4 %fusion.5 = f32[1024,2048]{1,0:T(8,128)S(1)} fusion(bf16[1024,352]{0,1:T(8,128)(2,1)S(1)} %get-tuple-element.23, bf16[352,2048]{1,0:T(8,128)(2,1)S(1)} %copy-done.1), kind=kOutput, calls=%fused_computation.15 | convolution fusion | flops 1476395008 | bytes 10551296 | tf_op jit(solution)/shard_map/dot_general | solution.py:322
  114.1 0.0 copy-done
  114.1 4.7 %add_convert_fusion.refs_3_ = bf16[1024,2048]{1,0:T(8,128)(2,1)} fusion(f32[1024,2048]{1,0:T(8,128)S(1)} %fusion.5, bf16[1024,352]{0,1:T(8,128)(2,1)S(1)} %get-tuple-element.22, bf16[352,2048]{1,0:T(8,128)(2,1)S(1)} %copy-done), kind=kOutput, calls=%fused_computation | convolution fusion | flops 1480589312 | bytes 14745600 | tf_op jit(solution)/shard_map/dot_general | solution.py:322
  118.8 79.7 %shard_map.85 = (bf16[3,1408,256]{2,1,0:T(8,128)(2,1)}, bf16[256,512]{1,0:T(8,128)(2,1)}) custom-call(bf16[352,2048]{1,0:T(8,128)(2,1)} %convolution_convert_fusion.2.refs_0_, bf16[352,2048]{1,0:T(8,128)(2,1)} %convolution_convert_fusion.1.refs_1_, bf16[352,2048]{1,0:T(8,128)(2,1)} %convolution_convert_fusion.refs_2_, bf16[1024,2048]{1,0:T(8,128)(2,1)} %add_convert_fusion.refs_3_), custom_call_target="tpu_custom_call" | custom-call | tf_op jit(solution)/shard_map/pallas_call | solution.py:326
  198.5 3.0 %bitcast_convert_fusion = (f32[1408,256]{1,0:T(8,128)}, f32[256,1408]{0,1:T(8,128)S(1)}, f32[256,1408]{0,1:T(8,128)S(1)}) fusion(bf16[3,1408,256]{2,1,0:T(8,128)(2,1)} %get-tuple-element.17), kind=kLoop, calls=%fused_computation.11 | loop fusion | flops 1081344 | bytes 6488064 | tf_op jit(solution)/shard_map/convert_element_type | solution.py:355
  201.5 1.5 copy.12
  203.1 0.0 copy-start.3
  203.1 1.5 copy.11
  204.6 0.0 copy-done.3
  204.6 0.7 copy.14
Async XLA Ops:
  0.6 2.3 %copy-start.2 = (bf16[256,1408]{1,0:T(8,128)(2,1)S(1)}, bf16[256,1408]{1,0:T(8,128)(2,1)}, u32[]{:S(2)}) copy-start(bf16[256,1408]{1,0:T(8,128)(2,1)} %param.8) | copy-start | bytes 2162692
  93.9 4.5 %copy-start.1 = (bf16[352,2048]{1,0:T(8,128)(2,1)S(1)}, bf16[352,2048]{1,0:T(8,128)(2,1)}, u32[]{:S(2)}) copy-start(bf16[352,2048]{1,0:T(8,128)(2,1)} %get-tuple-element.15) | copy-start | bytes 4325380
  93.9 4.5 %copy-start.4 = (bf16[1024,2048]{1,0:T(8,128)(2,1)S(1)}, bf16[1024,2048]{1,0:T(8,128)(2,1)}, u32[]{:S(2)}) copy-start(bf16[1024,2048]{1,0:T(8,128)(2,1)} %get-tuple-element.13) | copy-start | bytes 12582916
  98.4 2.2 %copy-start.5 = (bf16[1024,2048]{1,0:T(8,128)(2,1)S(1)}, bf16[1024,2048]{1,0:T(8,128)(2,1)}, u32[]{:S(2)}) copy-start(bf16[1024,2048]{1,0:T(8,128)(2,1)} %get-tuple-element.11) | copy-start | bytes 12582916
  98.4 2.6 %copy-start.6 = (bf16[352,2048]{1,0:T(8,128)(2,1)S(1)}, bf16[352,2048]{1,0:T(8,128)(2,1)}, u32[]{:S(2)}) copy-start(bf16[352,2048]{1,0:T(8,128)(2,1)} %get-tuple-element.12) | copy-start | bytes 4325380
  111.7 2.4 %copy-start = (bf16[352,2048]{1,0:T(8,128)(2,1)S(1)}, bf16[352,2048]{1,0:T(8,128)(2,1)}, u32[]{:S(2)}) copy-start(bf16[352,2048]{1,0:T(8,128)(2,1)} %get-tuple-element.14) | copy-start | bytes 4325380
  203.1 1.5 copy-start.3
where the time goes:
time: 209 us; the launch traced here: 205 us
  Pallas kernels  170 us (81%)
  matrix products  23.9 us (11%)
  local copies, waits for them, and re-layouts  8.15 us (4%)
  other arithmetic  3 us (1%)
    pallas_call x1, Pallas kernels, split_plan(): pl.pallas_call(functools.partial(gather_kernel, sizes), out_shape=[jax.Sh...  89.8 us
    pallas_call x1, Pallas kernels, split_plan(): pl.pallas_call(functools.partial(reduce_kernel, sizes), out_shape=[jax.Sh...  79.7 us
    dot_general x3, matrix products, contract_rows(): lax.dot_general(left, right, (((0,), (0,)), ((), ())), preferred_element_...  8.5 us
    dot_general x3, matrix products, contract_cols(): lax.dot_general(left, right, (((1,), (1,)), ((), ())), preferred_element_...  8.3 us
    unnamed x19, local copies, waits for them, and re-layouts  8.15 us
    dot_general x1, matrix products, split_plan(): jnp.dot(grad_up_pre, up_whole, preferred_element_type=jnp.float32)  4.69 us

commit v1 on v0

v1 whole, which is shorter than its diff:
```python
import functools

import jax
import jax.numpy as jnp
from jax import lax
from jax.experimental import pallas as pl
from jax.experimental.pallas import tpu as pltpu
from jax.sharding import PartitionSpec as P

MESH = pl.DeviceIdType.MESH
ANY = pl.BlockSpec(memory_space=pl.ANY)
VMEM = pl.BlockSpec(memory_space=pltpu.VMEM)
CORES = 2


def contract_rows(left, right):
    return lax.dot_general(
        left, right, (((0,), (0,)), ((), ())), preferred_element_type=jnp.float32
    )


def contract_cols(left, right):
    return lax.dot_general(
        left, right, (((1,), (1,)), ((), ())), preferred_element_type=jnp.float32
    )


def gathered_plan(inputs, cotangent, gate_weight, up_weight, down_weight):
    whole_inputs = lax.all_gather(inputs, "tp", axis=1, tiled=True)
    whole_cotangent = lax.all_gather(cotangent, "tp", axis=1, tiled=True)
    gate_whole = lax.all_gather(gate_weight, "fs", axis=0, tiled=True)
    up_whole = lax.all_gather(up_weight, "fs", axis=0, tiled=True)
    down_whole = lax.all_gather(down_weight, "fs", axis=1, tiled=True)
    gate_pre = jnp.dot(whole_inputs, gate_whole, preferred_element_type=jnp.float32)
    up_pre = jnp.dot(whole_inputs, up_whole, preferred_element_type=jnp.float32)
    grad_hidden = contract_cols(whole_cotangent, down_whole)
    hidden, grad_gate_pre, grad_up_pre = pointwise(gate_pre, up_pre, grad_hidden)
    pre_grads = jnp.concatenate([grad_gate_pre, grad_up_pre], axis=1)
    width = gate_weight.shape[1]
    partial_sum = contract_cols(grad_gate_pre, gate_whole) + contract_cols(grad_up_pre, up_whole)

    def scattered(values, axis, dim):
        return lax.psum_scatter(
            values.astype(jnp.bfloat16), axis, scatter_dimension=dim, tiled=True
        )

    grad_inputs = scattered(partial_sum, "tp", 1)
    expand = scattered(contract_rows(whole_inputs, pre_grads), "fs", 0).astype(jnp.float32)
    down = scattered(contract_rows(whole_cotangent, hidden), "fs", 0).astype(jnp.float32)
    return (grad_inputs, expand[:, :width], expand[:, width:], down.T)


def pointwise(gate_pre, up_pre, grad_hidden):
    gate_sig = jax.nn.sigmoid(gate_pre)
    gate_act = gate_pre * gate_sig
    hidden = (gate_act * up_pre).astype(jnp.bfloat16)
    grad_gate_pre = (grad_hidden * up_pre * gate_sig * (1.0 + gate_pre * (1.0 - gate_sig))).astype(
        jnp.bfloat16
    )
    grad_up_pre = (grad_hidden * gate_act).astype(jnp.bfloat16)
    return hidden, grad_gate_pre, grad_up_pre


def block(index, size):
    return pl.ds(pl.multiple_of(index * size, size), size)


class Place:
    def __init__(self, nz, ny, nx):
        self.nz, self.ny, self.nx = nz, ny, nx
        fs, tp = lax.axis_index("fs"), lax.axis_index("tp")
        self.fs, self.tp = fs, tp
        self.z, self.y = fs // ny, fs % ny
        self.x, self.c = tp // CORES, tp % CORES

    def by_z(self, dz):
        return {"fs": ((self.z + dz) % self.nz) * self.ny + self.y, "tp": self.tp}

    def by_y(self, dy):
        return {"fs": self.z * self.ny + (self.y + dy) % self.ny, "tp": self.tp}

    def by_x(self, dx):
        return {"fs": self.fs, "tp": ((self.x + dx) % self.nx) * CORES + self.c}

    def by_core(self):
        return {"fs": self.fs, "tp": self.x * CORES + 1 - self.c}

    def by_tp(self, dt):
        return {"fs": self.fs, "tp": (self.tp + dt) % (self.nx * CORES)}


def meet(partners):
    barrier = pltpu.get_barrier_semaphore()
    for partner in partners:
        pl.semaphore_signal(barrier, inc=1, device_id=partner, device_id_type=MESH)
    pl.semaphore_wait(barrier, len(partners))


class Copies:
    def __init__(self, send_sem, recv_sem):
        self.send_sem, self.recv_sem, self.made = send_sem, recv_sem, []

    def start(self, source, target, device):
        at = len(self.made)
        copy = pltpu.make_async_remote_copy(
            src_ref=source, dst_ref=target, send_sem=self.send_sem.at[at],
            recv_sem=self.recv_sem.at[at], device_id=device, device_id_type=MESH,
        )
        copy.start()
        self.made.append(copy)
        return copy


def flip(value, mask, nz):
    bit = 1
    while bit < nz:
        if mask & bit:
            value = value + bit - 2 * bit * ((value // bit) % 2)
        bit *= 2
    return value


def far_first(nz):
    return sorted(range(1, nz), key=lambda d: -min(d, nz - d))


def low_bits(nz):
    return [1 << at for at in range(nz.bit_length() - 1)]


def fused_kernel(sizes, halves, x_ref, c_ref, *refs):
    nz, ny, nx = sizes
    me = Place(*sizes)
    w_refs, (r, out) = refs[:3], refs[3:5]
    xf, cf, wg, wd, pre, hid, gs, rg, sg, ps, rc, sx, rx, vz, sz, rz, send_sem, recv_sem = refs[5:]
    tokens, features = x_ref.shape
    depth, units = w_refs[0].shape[1], w_refs[0].shape[0] // nz
    part = units // halves
    rows = tokens * nz
    meet(
        [me.by_z(d) for d in range(1, nz)]
        + [me.by_y(d) for d in range(1, ny)]
        + [me.by_x(d) for d in range(1, nx)]
        + [me.by_core()]
    )
    copies = Copies(send_sem, recv_sem)
    wholes = (xf, cf)
    by_x, sent_z, w_sent, token_last = {}, {}, {}, []
    w_last = [[] for _ in range(halves)]
    bits = low_bits(nz)[::-1]
    order = far_first(nz)

    def chunk(mask):
        return block(flip(me.z, mask, nz), tokens)

    def spot(whole, mask, tp):
        return whole.at[chunk(mask), block(tp, features)]

    def w_source(at, h, dz):
        start = pl.multiple_of(((me.z + dz) % nz) * units + h * part, 16)
        return w_refs[at].at[pl.ds(start, part), :]

    def w_spot(at, h, dz):
        column = block(((me.z - dz + nz) % nz) * ny + me.y, depth)
        if at < 2:
            return wg.at[pl.ds((2 * h + at) * part, part), column]
        return wd.at[pl.ds(h * part, part), column]

    def held(mask):
        return (x_ref, c_ref) if mask == 0 else [spot(whole, mask, me.tp) for whole in wholes]

    def pass_z(bit, mask):
        there = {"fs": flip(me.z, bit, nz) * ny + me.y, "tp": me.tp}
        sent_z[bit, mask] = [
            copies.start(source, spot(whole, mask, me.tp), there)
            for source, whole in zip(held(mask), wholes)
        ]

    def pass_tp(mask):
        for dx in range(1, nx):
            by_x[mask, dx] = [
                copies.start(source, spot(whole, mask, me.tp), me.by_x(dx))
                for source, whole in zip(held(mask), wholes)
            ]
        for source, whole in zip(held(mask), wholes):
            token_last.append(copies.start(source, spot(whole, mask, me.tp), me.by_core()))

    def pass_core(mask):
        for dx in range(1, nx):
            tp = ((me.x - dx + nx) % nx) * CORES + me.c
            for copy, whole in zip(by_x[mask, dx], wholes):
                copy.wait_recv()
                here = spot(whole, mask, tp)
                token_last.append(copies.start(here, here, me.by_core()))

    def send_w(h, dz):
        w_sent[h, dz] = [
            copies.start(w_source(at, h, dz), w_spot(at, h, 0), me.by_z(dz)) for at in range(3)
        ]

    def own_w(h):
        for at in range(3):
            for dy in range(1, ny):
                copy = copies.start(w_source(at, h, 0), w_spot(at, h, 0), me.by_y(dy))
                w_last[h].append(copy)

    def relay_w(h, dz):
        for at, copy in enumerate(w_sent[h, dz]):
            copy.wait_recv()
            here = w_spot(at, h, dz)
            w_last[h] += [copies.start(here, here, me.by_y(dy)) for dy in range(1, ny)]

    for bit in bits:
        pass_z(bit, 0)
    pass_tp(0)
    send_w(0, order[0])
    own_w(0)
    for held_ref, whole in zip((x_ref, c_ref), wholes):
        whole[chunk(0), block(me.tp, features)] = held_ref[...]
    for h in range(halves):
        for at in range(3):
            start = pl.multiple_of(me.z * units + h * part, 16)
            w_spot(at, h, 0)[...] = w_refs[at][pl.ds(start, part), :]
    masks = [0]
    for at, bit in enumerate(bits):
        for mask in list(masks):
            for copy in sent_z[bit, mask]:
                copy.wait_recv()
            masks.append(mask + bit)
            for lower in bits[at + 1 :]:
                pass_z(lower, mask + bit)
            pass_tp(mask + bit)
        if at == 0:
            for dz in order[1:]:
                send_w(0, dz)
            for h in range(1, halves):
                for dz in order:
                    send_w(h, dz)
                own_w(h)
    for mask in masks:
        pass_core(mask)
    for dz in order:
        relay_w(0, dz)
    for copy in token_last:
        copy.wait_recv()

    tile = min(256, rows)

    def forward(h):
        pair = pl.ds(2 * h * part, 2 * part)
        single = pl.ds(h * part, part)

        def step(at, carry):
            some = block(at, tile)
            both = contract_cols(wg[pair, :], xf[some, :])
            grad_hidden = contract_cols(wd[single, :], cf[some, :])
            hidden, gate, up = pointwise(both[:part], both[part:], grad_hidden)
            hid[single, some] = hidden
            pre[pl.ds(2 * h * part, part), some] = gate
            pre[pl.ds((2 * h + 1) * part, part), some] = up
            return carry

        lax.fori_loop(0, rows // tile, step, 0)

    waiting = []

    def release():
        while waiting:
            sink, source, target, device = waiting.pop(0)
            sink.append(copies.start(source, target, device))

    def grads(h, dz, y):
        columns = block(((me.z + dz) % nz) * ny + y, depth)
        pair = jnp.dot(
            pre[pl.ds(2 * h * part, 2 * part), :], xf[:, columns], preferred_element_type=jnp.float32
        )
        single = jnp.dot(
            hid[pl.ds(h * part, part), :], cf[:, columns], preferred_element_type=jnp.float32
        )
        return pair, single

    to_y, final = {}, []

    def give(h, dz):
        pair, single = grads(h, dz, (me.y + 1) % ny)
        release()
        gs[h, dz, pl.ds(0, 2 * part), :] = pair.astype(gs.dtype)
        gs[h, dz, pl.ds(2 * part, part), :] = single.astype(gs.dtype)
        to_y[h, dz] = []
        waiting.append((to_y[h, dz], gs.at[h, dz], rg.at[h, dz], me.by_y(1)))

    def settle(h, dz):
        pair, single = grads(h, dz, me.y)
        release()
        to_y[h, dz][0].wait_recv()
        pair += rg[h, dz, pl.ds(0, 2 * part), :].astype(jnp.float32)
        single += rg[h, dz, pl.ds(2 * part, part), :].astype(jnp.float32)
        target = sg.at[h, dz] if dz else r.at[me.z, h]
        target[pl.ds(0, 2 * part), :] = pair.astype(sg.dtype)
        target[pl.ds(2 * part, part), :] = single.astype(sg.dtype)
        if dz:
            waiting.append((final, sg.at[h, dz], r.at[me.z, h], me.by_z(dz)))

    def partial(mask, tp):
        return contract_rows(pre[:, chunk(mask)], wg[:, block(tp, features)])

    back = sorted(masks, key=lambda mask: [mask & bit == 0 for bit in low_bits(nz)])
    to_core, to_x = {}, {}

    def give_core(mask):
        for x in range(nx):
            values = partial(mask, x * CORES + 1 - me.c)
            release()
            ps[mask, x] = values.astype(ps.dtype)
        to_core[mask] = []
        waiting.append((to_core[mask], ps.at[mask], rc.at[mask], me.by_core()))

    def give_x(mask):
        there = (me.x + 1) % nx
        values = partial(mask, there * CORES + me.c)
        release()
        to_core[mask][0].wait_recv()
        sx[mask] = (values + rc[mask, there].astype(jnp.float32)).astype(sx.dtype)
        to_x[mask] = []
        waiting.append((to_x[mask], sx.at[mask], rx.at[mask], me.by_x(1)))
        values = partial(mask, me.tp)
        release()
        vz[mask] = values + rc[mask, me.x].astype(jnp.float32)

    for h in range(halves):
        for copy in w_last[h]:
            copy.wait_recv()
        forward(h)
        for dz in order + [0]:
            give(h, dz)
        release()
        if h + 1 < halves:
            for dz in order:
                relay_w(h + 1, dz)
        else:
            for mask in back:
                give_core(mask)
            release()
        for dz in order + [0]:
            settle(h, dz)
        release()
    for mask in back:
        give_x(mask)
    release()
    for mask in back:
        to_x[mask][0].wait_recv()
        vz[mask] += rx[mask].astype(jnp.float32)
    left = list(masks)
    for bit in low_bits(nz):
        moving = [mask for mask in left if mask & bit]
        left = [mask for mask in left if not mask & bit]
        there = {"fs": flip(me.z, bit, nz) * ny + me.y, "tp": me.tp}
        came = {}
        for mask in moving:
            sz[mask] = vz[mask].astype(sz.dtype)
        for mask in moving:
            came[mask - bit] = copies.start(sz.at[mask], rz.at[mask], there)
        for mask in left:
            came[mask].wait_recv()
            vz[mask] += rz[mask + bit].astype(jnp.float32)
    out[...] = vz[0].astype(out.dtype)
    for copy in final:
        copy.wait_recv()
    for copy in copies.made:
        copy.wait_send()


def finish_kernel(r, g_ref, gate, up, down, g_out, gate_buf, up_buf, down_buf, sem):
    nz, halves, triple, depth = r.shape
    part = triple // 3
    outs = [pltpu.make_async_copy(g_ref, g_out, sem.at[0])]
    outs[0].start()
    for z in range(nz):
        for h in range(halves):
            spot = pl.ds((z * halves + h) * part, part)
            down_buf[spot, :] = r[z, h, pl.ds(2 * part, part), :].astype(jnp.float32)
    outs.append(pltpu.make_async_copy(down_buf, down, sem.at[1]))
    outs[-1].start()
    for at, (buf, target) in enumerate(((gate_buf, gate), (up_buf, up))):
        whole = jnp.concatenate(
            [r[z, h, pl.ds(at * part, part), :] for z in range(nz) for h in range(halves)], axis=0
        )
        buf[...] = whole.astype(jnp.float32).T
        outs.append(pltpu.make_async_copy(buf, target, sem.at[2 + at]))
        outs[-1].start()
    for copy in outs:
        copy.wait()


def split_plan(sizes, inputs, cotangent, gate_weight, up_weight, down_weight):
    nz, ny, nx = sizes
    tokens, features = inputs.shape
    depth, width = gate_weight.shape
    units, rows, model = width // nz, tokens * nz, depth * nz * ny
    halves = 2 if units % 32 == 0 else 1
    part = units // halves
    dma, half, full = pltpu.SemaphoreType.DMA, jnp.bfloat16, jnp.float32
    count = 2 * (nz - 1 + 2 * nz * nx) + 3 * halves * (nz - 1 + nz * (ny - 1))
    count += halves * (2 * nz - 1) + 2 * nz + nz - 1
    settled, grad_inputs = pl.pallas_call(
        functools.partial(fused_kernel, sizes, halves),
        out_shape=[
            jax.ShapeDtypeStruct((nz, halves, 3 * part, depth), half),
            jax.ShapeDtypeStruct((tokens, features), half),
        ],
        in_specs=[VMEM] * 5,
        out_specs=[VMEM, VMEM],
        scratch_shapes=[
            pltpu.VMEM((rows, model), half),
            pltpu.VMEM((rows, model), half),
            pltpu.VMEM((2 * units, model), half),
            pltpu.VMEM((units, model), half),
            pltpu.VMEM((2 * units, rows), half),
            pltpu.VMEM((units, rows), half),
            pltpu.VMEM((halves, nz, 3 * part, depth), half),
            pltpu.VMEM((halves, nz, 3 * part, depth), half),
            pltpu.VMEM((halves, nz, 3 * part, depth), half),
            pltpu.VMEM((nz, nx, tokens, features), half),
            pltpu.VMEM((nz, nx, tokens, features), half),
            pltpu.VMEM((nz, tokens, features), half),
            pltpu.VMEM((nz, tokens, features), half),
            pltpu.VMEM((nz, tokens, features), full),
            pltpu.VMEM((nz, tokens, features), half),
            pltpu.VMEM((nz, tokens, features), half),
            dma((count,)),
            dma((count,)),
        ],
        compiler_params=pltpu.CompilerParams(
            collective_id=0, has_side_effects=True, vmem_limit_bytes=60 * 2**20
        ),
    )(inputs, cotangent, gate_weight.T, up_weight.T, down_weight)
    gate, up, down, grad_inputs = pl.pallas_call(
        finish_kernel,
        out_shape=[
            jax.ShapeDtypeStruct((depth, width), full),
            jax.ShapeDtypeStruct((depth, width), full),
            jax.ShapeDtypeStruct((width, depth), full),
            jax.ShapeDtypeStruct((tokens, features), half),
        ],
        in_specs=[VMEM] * 2,
        out_specs=[ANY] * 4,
        scratch_shapes=[
            pltpu.VMEM((depth, width), full),
            pltpu.VMEM((depth, width), full),
            pltpu.VMEM((width, depth), full),
            dma((4,)),
        ],
    )(settled, grad_inputs)
    return grad_inputs, gate, up, down


def solution(mesh):
    n_fs, n_tp = mesh.shape["fs"], mesh.shape["tp"]
    nx = max(1, n_tp // CORES)
    ny = nx
    nz = n_fs // ny

    def per_device(inputs, cotangent, gate_weight, up_weight, down_weight):
        arrays = (inputs, cotangent, gate_weight, up_weight, down_weight)
        depth, width = gate_weight.shape
        fits = n_tp == nx * CORES and nz > 1 and ny > 1 and n_fs == nz * ny
        fits = fits and nz & (nz - 1) == 0 and nx == 2
        tiles = depth % 128 == 0 and inputs.shape[1] % 128 == 0 and inputs.shape[0] % 16 == 0
        if fits and tiles and width % (16 * nz) == 0:
            return split_plan((nz, ny, nx), *arrays)
        return gathered_plan(*arrays)

    return jax.shard_map(
        per_device,
        mesh=mesh,
        in_specs=(P("fs", "tp"), P("fs", "tp"), P("fs", "tp"), P("fs", "tp"), P("tp", "fs")),
        out_specs=(P("fs", "tp"), P("fs", "tp"), P("fs", "tp"), P("tp", "fs")),
        check_vma=False,
    )
```

time: 209 us -> 199 us (0.952); the launches traced: 205 us -> 198 us
  Pallas kernels: 170 us -> 194 us
  matrix products: 23.9 us -> 0 us
  local copies, waits for them, and re-layouts: 8.15 us -> 3.45 us
  other arithmetic: 3 us -> 0 us
    pallas_call x2, Pallas kernels: 170 us -> 194 us  [the longest x1 190 us: split_plan(): pl.pallas_call(functools.partial(fused_kernel, sizes, halves), out_shape=...]
    dot_general x8 -> x0, matrix products: 23.9 us -> none  [the longest x3 8.5 us: contract_rows(): lax.dot_general(left, right, (((0,), (0,)), ((), ())), preferred_element_...]
    unnamed x19 -> x4, local copies, waits for them, and re-layouts: 8.15 us -> 3.45 us
    convert_element_type x1 -> x0, other arithmetic: 3 us -> none  [split_plan(): settled[2].astype(jnp.float32)]
where the time goes in v1:
time: 199 us; the launch traced here: 198 us
  Pallas kernels  194 us (97%)
  local copies, waits for them, and re-layouts  3.45 us (2%)
    pallas_call x1, Pallas kernels, split_plan(): pl.pallas_call(functools.partial(fused_kernel, sizes, halves), out_shape=...  190 us
    pallas_call x1, Pallas kernels, split_plan(): pl.pallas_call(finish_kernel, out_shape=[jax.ShapeDtypeStruct((depth, wid...  4.19 us

profile of v1, /device:TPU:0, one launch (start us, length us, event | category | flops | bytes accessed | tf_op | source)
XLA Modules:
  0.0 198.2 jit_solution(2282718887072471831)
XLA Ops:
  0.6 0.0 copy-start
  0.6 2.3 %copy.9 = bf16[256,1408]{0,1:T(8,128)(2,1)} copy(bf16[256,1408]{1,0:T(8,128)(2,1)} %param.7) | data formatting | bytes 1441792 | tf_op args[2]
  3.0 0.0 copy-done
  3.0 1.1 copy.10
  4.1 189.7 %shard_map.84 = (bf16[4,2,528,256]{3,2,1,0:T(8,128)(2,1)}, bf16[256,512]{1,0:T(8,128)(2,1)}) custom-call(bf16[256,512]{1,0:T(8,128)(2,1)} %x_ref.1, bf16[256,512]{1,0:T(8,128)(2,1)} %c_ref.1, bf16[1408,256]{1,0:T(8,128)(2,1)} %bitcast.2, bf16[1408,256]{1,0:T(8,128)(2,1)} %bitcast.3, bf16[1408,256]{1,0:T(8,128)(2,1)} %refs_2_.1), custom_call_target="tpu_custom_call" | custom-call | tf_op jit(solution)/shard_map/pallas_call | solution.py:405
  193.8 4.2 %shard_map.85 = (f32[256,1408]{1,0:T(8,128)}, f32[256,1408]{1,0:T(8,128)}, f32[1408,256]{1,0:T(8,128)}, bf16[256,512]{1,0:T(8,128)(2,1)}) custom-call(bf16[4,2,528,256]{3,2,1,0:T(8,128)(2,1)} %get-tuple-element.10.r, bf16[256,512]{1,0:T(8,128)(2,1)} %get-tuple-element.11.g_ref), custom_call_target="tpu_custom_call" | custom-call | tf_op jit(solution)/shard_map/pallas_call | solution.py:437
Async XLA Ops:
  0.6 2.3 %copy-start = (bf16[256,1408]{1,0:T(8,128)(2,1)S(1)}, bf16[256,1408]{1,0:T(8,128)(2,1)}, u32[]{:S(2)}) copy-start(bf16[256,1408]{1,0:T(8,128)(2,1)} %param.8) | copy-start | bytes 2162692

commit v2 on v1

--- a/solution.py
+++ b/solution.py
@@ -128,121 +128,157 @@
     return [1 << at for at in range(nz.bit_length() - 1)]
 
 
-def fused_kernel(sizes, halves, x_ref, c_ref, *refs):
+def fused_kernel(sizes, halves, *refs):
     nz, ny, nx = sizes
     me = Place(*sizes)
-    w_refs, (r, out) = refs[:3], refs[3:5]
-    xf, cf, wg, wd, pre, hid, gs, rg, sg, ps, rc, sx, rx, vz, sz, rz, send_sem, recv_sem = refs[5:]
-    tokens, features = x_ref.shape
-    depth, units = w_refs[0].shape[1], w_refs[0].shape[0] // nz
+    ins, (r, out), (raw, turned, xf, cf, wg, wd) = refs[:5], refs[5:7], refs[7:13]
+    pre, hid, gs, rg, sg, ps, rc, sx, rx, vz, sz, rz, send_sem, recv_sem, own_sem = refs[13:]
+    tokens, features = ins[0].shape
+    depth, units = ins[2].shape[0], ins[2].shape[1] // nz
     part = units // halves
     rows = tokens * nz
-    meet(
-        [me.by_z(d) for d in range(1, nz)]
-        + [me.by_y(d) for d in range(1, ny)]
-        + [me.by_x(d) for d in range(1, nx)]
-        + [me.by_core()]
-    )
+    scope = jax.named_scope
     copies = Copies(send_sem, recv_sem)
     wholes = (xf, cf)
     by_x, sent_z, w_sent, token_last = {}, {}, {}, []
     w_last = [[] for _ in range(halves)]
-    bits = low_bits(nz)[::-1]
-    order = far_first(nz)
+    bits = low_bits(nz)
+    order = sorted(range(1, nz), key=lambda mask: (mask & -mask == 1, mask))
+    order = sorted(order, key=lambda mask: mask < nz // 2)
 
     def chunk(mask):
         return block(flip(me.z, mask, nz), tokens)
 
-    def spot(whole, mask, tp):
-        return whole.at[chunk(mask), block(tp, features)]
-
-    def w_source(at, h, dz):
-        start = pl.multiple_of(((me.z + dz) % nz) * units + h * part, 16)
-        return w_refs[at].at[pl.ds(start, part), :]
-
-    def w_spot(at, h, dz):
-        column = block(((me.z - dz + nz) % nz) * ny + me.y, depth)
+    def by_flip(mask):
+        return {"fs": flip(me.z, mask, nz) * ny + me.y, "tp": me.tp}
+
+    def spot(at, mask, tp):
+        return wholes[at].at[chunk(mask), block(tp, features)]
+
+    def w_source(at, h, mask):
+        start = pl.multiple_of(flip(me.z, mask, nz) * units + h * part, 16)
+        return turned.at[at, pl.ds(start, part), :]
+
+    def w_spot(at, h, mask):
+        column = block(flip(me.z, mask, nz) * ny + me.y, depth)
         if at < 2:
             return wg.at[pl.ds((2 * h + at) * part, part), column]
         return wd.at[pl.ds(h * part, part), column]
 
-    def held(mask):
-        return (x_ref, c_ref) if mask == 0 else [spot(whole, mask, me.tp) for whole in wholes]
-
-    def pass_z(bit, mask):
-        there = {"fs": flip(me.z, bit, nz) * ny + me.y, "tp": me.tp}
-        sent_z[bit, mask] = [
-            copies.start(source, spot(whole, mask, me.tp), there)
-            for source, whole in zip(held(mask), wholes)
-        ]
-
-    def pass_tp(mask):
+    fetch = [pltpu.make_async_copy(ins[at], spot(at, 0, me.tp), own_sem.at[at]) for at in range(2)]
+    fetch += [pltpu.make_async_copy(ins[2 + at], raw.at[at], own_sem.at[2 + at]) for at in range(2)]
+    fetch.append(pltpu.make_async_copy(ins[4], turned.at[2], own_sem.at[4]))
+    for copy in fetch:
+        copy.start()
+    with scope("meet"):
+        meet(
+            [me.by_z(d) for d in range(1, nz)]
+            + [me.by_y(d) for d in range(1, ny)]
+            + [me.by_x(d) for d in range(1, nx)]
+            + [me.by_core()]
+        )
+
+    def pass_z(bit, mask, at):
+        here = spot(at, mask, me.tp)
+        sent_z[bit, mask, at] = copies.start(here, here, by_flip(bit))
+
+    def pass_tp(mask, at):
+        here = spot(at, mask, me.tp)
         for dx in range(1, nx):
-            by_x[mask, dx] = [
-                copies.start(source, spot(whole, mask, me.tp), me.by_x(dx))
-                for source, whole in zip(held(mask), wholes)
-            ]
-        for source, whole in zip(held(mask), wholes):
-            token_last.append(copies.start(source, spot(whole, mask, me.tp), me.by_core()))
-
-    def pass_core(mask):
+            by_x[mask, dx, at] = copies.start(here, here, me.by_x(dx))
+        token_last.append(copies.start(here, here, me.by_core()))
+
+    def pass_core(mask, at):
         for dx in range(1, nx):
             tp = ((me.x - dx + nx) % nx) * CORES + me.c
-            for copy, whole in zip(by_x[mask, dx], wholes):
-                copy.wait_recv()
-                here = spot(whole, mask, tp)
-                token_last.append(copies.start(here, here, me.by_core()))
-
-    def send_w(h, dz):
-        w_sent[h, dz] = [
-            copies.start(w_source(at, h, dz), w_spot(at, h, 0), me.by_z(dz)) for at in range(3)
+            by_x[mask, dx, at].wait_recv()
+            here = spot(at, mask, tp)
+            token_last.append(copies.start(here, here, me.by_core()))
+
+    def take_tokens(bit, mask, at):
+        sent_z[bit, mask, at].wait_recv()
+        for lower in bits:
+            if lower < bit and mask % (2 * bit) == 0:
+                pass_z(lower, mask + bit, at)
+        pass_tp(mask + bit, at)
+
+    def send_w(h, mask):
+        w_sent[h, mask] = [
+            copies.start(w_source(at, h, mask), w_spot(at, h, 0), by_flip(mask))
+            for at in range(3)
         ]
 
-    def own_w(h):
-        for at in range(3):
-            for dy in range(1, ny):
-                copy = copies.start(w_source(at, h, 0), w_spot(at, h, 0), me.by_y(dy))
-                w_last[h].append(copy)
-
-    def relay_w(h, dz):
-        for at, copy in enumerate(w_sent[h, dz]):
+    def own_w(h, at):
+        for dy in range(1, ny):
+            w_last[h].append(copies.start(w_source(at, h, 0), w_spot(at, h, 0), me.by_y(dy)))
+
+    def relay_w(h, mask):
+        for at, copy in enumerate(w_sent[h, mask]):
             copy.wait_recv()
-            here = w_spot(at, h, dz)
+            here = w_spot(at, h, mask)
             w_last[h] += [copies.start(here, here, me.by_y(dy)) for dy in range(1, ny)]
 
-    for bit in bits:
-        pass_z(bit, 0)
-    pass_tp(0)
+    def do(what, *key):
+        with scope(f"{what.__name__}#" + "#".join(str(k) for k in key)):
+            what(*key)
+
+    for at in range(2):
+        fetch[at].wait()
+        for bit in bits:
+            pass_z(bit, 0, at)
+        pass_tp(0, at)
+    fetch[4].wait()
+    for h in range(halves):
+        own_w(h, 2)
+    with scope("turn"):
+        for at in range(2):
+            fetch[2 + at].wait()
+            for start in range(0, units * nz, 128):
+                some = pl.ds(start, 128)
+                turned[at, some, :] = raw[at, :, some].T
+    for h in range(halves):
+        for at in range(2):
+            own_w(h, at)
     send_w(0, order[0])
-    own_w(0)
-    for held_ref, whole in zip((x_ref, c_ref), wholes):
-        whole[chunk(0), block(me.tp, features)] = held_ref[...]
     for h in range(halves):
         for at in range(3):
             start = pl.multiple_of(me.z * units + h * part, 16)
-            w_spot(at, h, 0)[...] = w_refs[at][pl.ds(start, part), :]
-    masks = [0]
-    for at, bit in enumerate(bits):
-        for mask in list(masks):
-            for copy in sent_z[bit, mask]:
-                copy.wait_recv()
-            masks.append(mask + bit)
-            for lower in bits[at + 1 :]:
-                pass_z(lower, mask + bit)
-            pass_tp(mask + bit)
-        if at == 0:
-            for dz in order[1:]:
-                send_w(0, dz)
-            for h in range(1, halves):
-                for dz in order:
-                    send_w(h, dz)
-                own_w(h)
-    for mask in masks:
-        pass_core(mask)
-    for dz in order:
-        relay_w(0, dz)
-    for copy in token_last:
-        copy.wait_recv()
+            w_spot(at, h, 0)[...] = turned[at, pl.ds(start, part), :]
+    later = []
+    for mask in range(1, nz):
+        later += [(bit, mask) for bit in bits if bit < (mask & -mask)]
+    cores = [(0, 0), (0, 1)]
+    for at in range(2):
+        for bit in bits:
+            do(take_tokens, bit, 0, at)
+            cores.append((bit, at))
+        for key in cores[:2]:
+            do(pass_core, *key)
+        cores = cores[2:]
+    for mask in order[1:]:
+        send_w(0, mask)
+    for key in cores[:1]:
+        do(pass_core, *key)
+    cores = cores[1:]
+    for bit, mask in later:
+        do(take_tokens, bit, mask, 0)
+        cores.append((mask + bit, 0))
+    do(relay_w, 0, order[0])
+    for bit, mask in later:
+        do(take_tokens, bit, mask, 1)
+        cores.append((mask + bit, 1))
+    for h in range(1, halves):
+        for mask in order:
+            send_w(h, mask)
+    for key in cores[:-2]:
+        do(pass_core, *key)
+    for mask in order[1:]:
+        do(relay_w, 0, mask)
+    for key in cores[-2:]:
+        do(pass_core, *key)
+    with scope("wait_tokens"):
+        for copy in token_last:
+            copy.wait_recv()
 
     tile = min(256, rows)
 
@@ -269,8 +305,8 @@
             sink, source, target, device = waiting.pop(0)
             sink.append(copies.start(source, target, device))
 
-    def grads(h, dz, y):
-        columns = block(((me.z + dz) % nz) * ny + y, depth)
+    def grads(h, mask, y):
+        columns = block(flip(me.z, mask, nz) * ny + y, depth)
         pair = jnp.dot(
             pre[pl.ds(2 * h * part, 2 * part), :], xf[:, columns], preferred_element_type=jnp.float32
         )
@@ -281,30 +317,30 @@
 
     to_y, final = {}, []
 
-    def give(h, dz):
-        pair, single = grads(h, dz, (me.y + 1) % ny)
-        release()
-        gs[h, dz, pl.ds(0, 2 * part), :] = pair.astype(gs.dtype)
-        gs[h, dz, pl.ds(2 * part, part), :] = single.astype(gs.dtype)
-        to_y[h, dz] = []
-        waiting.append((to_y[h, dz], gs.at[h, dz], rg.at[h, dz], me.by_y(1)))
-
-    def settle(h, dz):
-        pair, single = grads(h, dz, me.y)
-        release()
-        to_y[h, dz][0].wait_recv()
-        pair += rg[h, dz, pl.ds(0, 2 * part), :].astype(jnp.float32)
-        single += rg[h, dz, pl.ds(2 * part, part), :].astype(jnp.float32)
-        target = sg.at[h, dz] if dz else r.at[me.z, h]
-        target[pl.ds(0, 2 * part), :] = pair.astype(sg.dtype)
-        target[pl.ds(2 * part, part), :] = single.astype(sg.dtype)
-        if dz:
-            waiting.append((final, sg.at[h, dz], r.at[me.z, h], me.by_z(dz)))
+    def give(h, mask):
+        pair, single = grads(h, mask, (me.y + 1) % ny)
+        release()
+        gs[h, mask, pl.ds(0, 2 * part), :] = pair.astype(gs.dtype)
+        gs[h, mask, pl.ds(2 * part, part), :] = single.astype(gs.dtype)
+        to_y[h, mask] = []
+        waiting.append((to_y[h, mask], gs.at[h, mask], rg.at[h, mask], me.by_y(1)))
+
+    def settle(h, mask):
+        pair, single = grads(h, mask, me.y)
+        release()
+        with scope("wait_y"):
+            to_y[h, mask][0].wait_recv()
+        pair += rg[h, mask, pl.ds(0, 2 * part), :].astype(jnp.float32)
+        single += rg[h, mask, pl.ds(2 * part, part), :].astype(jnp.float32)
+        sg[h, mask, pl.ds(0, 2 * part), :] = pair.astype(sg.dtype)
+        sg[h, mask, pl.ds(2 * part, part), :] = single.astype(sg.dtype)
+        if mask:
+            waiting.append((final, sg.at[h, mask], r.at[me.z, h], by_flip(mask)))
 
     def partial(mask, tp):
         return contract_rows(pre[:, chunk(mask)], wg[:, block(tp, features)])
 
-    back = sorted(masks, key=lambda mask: [mask & bit == 0 for bit in low_bits(nz)])
+    back = sorted(range(nz), key=lambda mask: [mask & bit == 0 for bit in bits])
     to_core, to_x = {}, {}
 
     def give_core(mask):
@@ -327,47 +363,89 @@
         release()
         vz[mask] = values + rc[mask, me.x].astype(jnp.float32)
 
-    for h in range(halves):
-        for copy in w_last[h]:
-            copy.wait_recv()
-        forward(h)
-        for dz in order + [0]:
-            give(h, dz)
-        release()
-        if h + 1 < halves:
-            for dz in order:
-                relay_w(h + 1, dz)
-        else:
-            for mask in back:
-                give_core(mask)
-            release()
-        for dz in order + [0]:
-            settle(h, dz)
-        release()
-    for mask in back:
-        give_x(mask)
-    release()
-    for mask in back:
+    def ready(h):
+        release()
+        with scope(f"wait_w#h={h}"):
+            for copy in w_last[h]:
+                copy.wait_recv()
+        with scope(f"forward#h={h}"):
+            forward(h)
+
+    def take_x(mask):
+        release()
         to_x[mask][0].wait_recv()
         vz[mask] += rx[mask].astype(jnp.float32)
-    left = list(masks)
-    for bit in low_bits(nz):
-        moving = [mask for mask in left if mask & bit]
-        left = [mask for mask in left if not mask & bit]
-        there = {"fs": flip(me.z, bit, nz) * ny + me.y, "tp": me.tp}
-        came = {}
-        for mask in moving:
-            sz[mask] = vz[mask].astype(sz.dtype)
-        for mask in moving:
-            came[mask - bit] = copies.start(sz.at[mask], rz.at[mask], there)
+
+    came = {}
+
+    def send_z(bit, mask):
+        sz[mask] = vz[mask].astype(sz.dtype)
+        came[bit, mask - bit] = []
+        waiting.append((came[bit, mask - bit], sz.at[mask], rz.at[mask], by_flip(bit)))
+
+    def take_z(bit, mask):
+        release()
+        came[bit, mask][0].wait_recv()
+        vz[mask] += rz[mask + bit].astype(jnp.float32)
+
+    last = halves - 1
+    for h in range(last):
+        ready(h)
+        for at, mask in enumerate(order):
+            do(give, h, mask)
+            release()
+            do(relay_w, h + 1, mask)
+            if at:
+                do(settle, h, order[at - 1])
+    ready(last)
+    for mask in order:
+        do(give, last, mask)
+    for mask in back:
+        do(give_core, mask)
+    for mask in back:
+        do(give_x, mask)
+    steps = [(settle, h, order[-1]) for h in range(last)]
+    steps += [(settle, last, mask) for mask in order]
+    for h in range(halves):
+        steps += [(give, h, 0)]
+    steps += [(settle, h, 0) for h in range(halves)]
+
+    def step(count=1):
+        for _ in range(min(count, len(steps))):
+            do(*steps.pop(0))
+        release()
+
+    step(2)
+    left = list(back)
+    for mask in back:
+        do(take_x, mask)
+        if mask & 1:
+            do(send_z, 1, mask)
+        step()
+    left = [mask for mask in back if not mask & 1]
+    for at, bit in enumerate(bits):
+        higher = bits[at + 1 :]
         for mask in left:
-            came[mask].wait_recv()
-            vz[mask] += rz[mask + bit].astype(jnp.float32)
+            do(take_z, bit, mask)
+            if higher and mask & higher[0]:
+                do(send_z, higher[0], mask)
+            step()
+        left = [mask for mask in left if not (higher and mask & higher[0])]
+    step(len(steps))
+    local = [
+        pltpu.make_async_copy(sg.at[h, 0], r.at[me.z, h], own_sem.at[h]) for h in range(halves)
+    ]
+    for copy in local:
+        copy.start()
     out[...] = vz[0].astype(out.dtype)
-    for copy in final:
-        copy.wait_recv()
-    for copy in copies.made:
-        copy.wait_send()
+    with scope("wait_final"):
+        for copy in final:
+            copy.wait_recv()
+    with scope("wait_sends"):
+        for copy in copies.made:
+            copy.wait_send()
+        for copy in local:
+            copy.wait()
 
 
 def finish_kernel(r, g_ref, gate, up, down, g_out, gate_buf, up_buf, down_buf, sem):
@@ -408,9 +486,11 @@
             jax.ShapeDtypeStruct((nz, halves, 3 * part, depth), half),
             jax.ShapeDtypeStruct((tokens, features), half),
         ],
-        in_specs=[VMEM] * 5,
-        out_specs=[VMEM, VMEM],
+        in_specs=[ANY] * 5,
+        out_specs=[ANY, VMEM],
         scratch_shapes=[
+            pltpu.VMEM((2, depth, width), half),
+            pltpu.VMEM((3, width, depth), half),
             pltpu.VMEM((rows, model), half),
             pltpu.VMEM((rows, model), half),
             pltpu.VMEM((2 * units, model), half),
@@ -429,11 +509,12 @@
             pltpu.VMEM((nz, tokens, features), half),
             dma((count,)),
             dma((count,)),
+            dma((5,)),
         ],
         compiler_params=pltpu.CompilerParams(
             collective_id=0, has_side_effects=True, vmem_limit_bytes=60 * 2**20
         ),
-    )(inputs, cotangent, gate_weight.T, up_weight.T, down_weight)
+    )(inputs, cotangent, gate_weight, up_weight, down_weight)
     gate, up, down, grad_inputs = pl.pallas_call(
         finish_kernel,
         out_shape=[

time: 199 us -> 166 us (0.83)
  Pallas kernels: 194 us -> 164 us
  local copies, waits for them, and re-layouts: 3.45 us -> 0 us
    pallas_call x1, Pallas kernels: 190 us -> 160 us  [split_plan(): pl.pallas_call(functools.partial(fused_kernel, sizes, halves), out_shape=...]
    unnamed x4 -> x0, local copies, waits for them, and re-layouts: 3.45 us -> none
where the time goes in v2:
time: 166 us; the launch traced here: 165 us
  Pallas kernels  164 us (99%)
    pallas_call x1, Pallas kernels, split_plan(): pl.pallas_call(functools.partial(fused_kernel, sizes, halves), out_shape=...  160 us
    pallas_call x1, Pallas kernels, split_plan(): pl.pallas_call(finish_kernel, out_shape=[jax.ShapeDtypeStruct((depth, wid...  4.19 us

profile of v2, /device:TPU:0, one launch (start us, length us, event | category | flops | bytes accessed | tf_op | source)
XLA Modules:
  0.0 165.1 jit_solution(16352131448442564193)
XLA Ops:
  0.6 160.1 %shard_map.84 = (bf16[4,2,528,256]{3,2,1,0:T(8,128)(2,1)}, bf16[256,512]{1,0:T(8,128)(2,1)}) custom-call(bf16[256,512]{1,0:T(8,128)(2,1)} %refs_0_.1, bf16[256,512]{1,0:T(8,128)(2,1)} %refs_1_.1, bf16[256,1408]{1,0:T(8,128)(2,1)} %refs_2_.1, bf16[256,1408]{1,0:T(8,128)(2,1)} %refs_3_.1, bf16[1408,256]{1,0:T(8,128)(2,1)} %refs_4_.1), custom_call_target="tpu_custom_call" | custom-call | tf_op jit(solution)/shard_map/pallas_call | solution.py:483
  160.8 4.2 %shard_map.85 = (f32[256,1408]{1,0:T(8,128)}, f32[256,1408]{1,0:T(8,128)}, f32[1408,256]{1,0:T(8,128)}, bf16[256,512]{1,0:T(8,128)(2,1)}) custom-call(bf16[4,2,528,256]{3,2,1,0:T(8,128)(2,1)} %get-tuple-element.10.r, bf16[256,512]{1,0:T(8,128)(2,1)} %get-tuple-element.11.g_ref), custom_call_target="tpu_custom_call" | custom-call | tf_op jit(solution)/shard_map/pallas_call | solution.py:518
